TPU v7x, 32 devices: a whole 2x2x4 slice. The times are simulated.
32 devices in a mesh: ep: 4 (over y, x), tp: 8 (over z, core).
Axes of the slice: x: 2, y: 2, z: 4, core: 2. Of those that a mesh axis runs over, the one named last changes fastest.
Arguments:
- tokens: bfloat16 [1024, 1024], P(('ep', 'tp')), may hold values from -6 to 6
- norm_gain: float32 [1024], replicated, may hold values from 0.5 to 1.5
- routing: int32 [1024, 2], P('ep'), may hold values from 0 to 7, as said below
- gate_share: float32 [1024, 2], P('ep'), may hold values from 0.5 to 1.5
- w_gate: bfloat16 [8, 1024, 256], P('ep', None, 'tp'), may hold values from -0.1875 to 0.1875
- w_up: bfloat16 [8, 1024, 256], P('ep', None, 'tp'), may hold values from -0.1875 to 0.1875
- w_down: bfloat16 [8, 256, 1024], P('ep', 'tp'), may hold values from -0.375 to 0.375
Outputs:
- mixed_out: bfloat16 [1024, 1024], P('ep', 'tp')
Inputs may be any that keep to these rules, and one draw needn't show every extreme that they name: `routing`: each row names two different experts whose ids lie in the same block of 2 consecutive ids. In each aligned block of 256 rows (the tokens of one index of ep) no expert is named by more than 128 rows, and some expert is named by exactly 128.
All inputs are finite; a program needn't handle non-finite values.
Results may differ from a plain program's by a relative error of at most 0.0015.
Values may be sent and summed in bfloat16 or wider, within the bound.
A program may use at most 64 MiB of HBM per device.

v0:
```python
import jax
import jax.numpy as jnp
from jax import lax
from jax.sharding import PartitionSpec as P

epsilon = 1e-06


def norm_rows(tokens, norm_gain):
    as_float = tokens.astype(jnp.float32)
    scaled = as_float * lax.rsqrt(jnp.mean(as_float * as_float, axis=-1, keepdims=True) + epsilon)
    return (scaled * norm_gain.astype(jnp.float32)).astype(jnp.bfloat16)


def fill_buffer(group, flat_target, slots, model_width):
    buffer = jnp.zeros((slots, model_width), jnp.bfloat16)
    return buffer.at[flat_target].set(jnp.repeat(group, 2, axis=0))


def body(tokens, norm_gain, routing, gate_share, w_gate, w_up, w_down):
    ep_size = lax.axis_size("ep")
    tp_size = lax.axis_size("tp")
    local_experts = w_gate.shape[0]
    experts = local_experts * ep_size
    group_rows = routing.shape[0]
    capacity = group_rows * 4 // experts
    model_width = tokens.shape[1]
    columns = model_width // tp_size
    normed = norm_rows(tokens, norm_gain)
    onehot = (routing[:, :, None] == jnp.arange(experts, dtype=jnp.int32)[None, None, :]).astype(
        jnp.int32
    )
    flat_hot = onehot.reshape(group_rows * 2, experts)
    ranking = jnp.cumsum(flat_hot, axis=0) - 1
    slot_pos = jnp.sum(ranking * flat_hot, axis=1).reshape(group_rows, 2)
    target = (routing * capacity + slot_pos).astype(jnp.int32)
    flat_target = target.reshape(-1)
    slice_len = capacity // tp_size
    tp_index = lax.axis_index("tp")
    group = lax.all_gather(normed, "tp", axis=0, tiled=True)
    buffer = fill_buffer(group, flat_target, experts * capacity, model_width)
    shaped = buffer.reshape(ep_size, local_experts, capacity, model_width)
    mine = lax.dynamic_slice_in_dim(shaped, tp_index * slice_len, slice_len, 2)
    mine = mine.reshape(ep_size, local_experts * slice_len, model_width)
    landed = lax.all_to_all(mine, "ep", split_axis=0, concat_axis=0, tiled=True)
    landed = landed.reshape(ep_size, local_experts, slice_len, model_width).transpose(1, 0, 2, 3)
    landed = landed.reshape(local_experts, ep_size * slice_len, model_width)
    full_gate, full_up, full_down = (
        lax.all_gather(w_gate, "tp", axis=2, tiled=True),
        lax.all_gather(w_up, "tp", axis=2, tiled=True),
        lax.all_gather(w_down, "tp", axis=1, tiled=True),
    )
    gate_sum = jnp.einsum("erd,edh->erh", landed, full_gate, preferred_element_type=jnp.float32)
    up_sum = jnp.einsum("erd,edh->erh", landed, full_up, preferred_element_type=jnp.float32)
    hidden = (jax.nn.silu(gate_sum) * up_sum).astype(jnp.bfloat16)
    produced = jnp.einsum(
        "erh,ehd->erd", hidden, full_down, preferred_element_type=jnp.float32
    ).astype(jnp.bfloat16)
    produced = produced.reshape(local_experts, ep_size, slice_len, model_width)
    blocks = lax.all_to_all(produced, "tp", split_axis=3, concat_axis=2, tiled=True)
    leaving = blocks.transpose(1, 0, 2, 3).reshape(ep_size, local_experts * capacity, columns)
    returned = lax.all_to_all(leaving, "ep", split_axis=0, concat_axis=0, tiled=True).reshape(
        experts * capacity, columns
    )
    picked_out = returned[target]
    mixed_out = jnp.sum(gate_share[:, :, None] * picked_out.astype(jnp.float32), axis=1)
    return mixed_out.astype(jnp.bfloat16)


def solution(mesh):
    return jax.shard_map(
        body,
        mesh=mesh,
        in_specs=(
            P(("ep", "tp"), None),
            P(),
            P("ep", None),
            P("ep", None),
            P("ep", None, "tp"),
            P("ep", None, "tp"),
            P("ep", "tp", None),
        ),
        out_specs=P("ep", "tp"),
        check_vma=False,
    )
```

profile of v0, /device:TPU:0, one launch (start us, length us, event | category | flops | bytes accessed | tf_op | source)
XLA Modules:
  0.0 124.2 jit_solution(3098279486913121579)
XLA Ops:
  6.5 0.7 all-gather.4.cloned.1.call-update
  7.3 0.7 all-gather.6.cloned.1.call-update
  8.1 0.7 all-gather.8.cloned.1.call-update
  8.7 0.8 copy.34
  9.6 0.1 eq.30
  9.7 0.1 eq.26
  9.9 1.1 reduce-window.6
  11.0 0.2 slice_reduce_fusion
  11.4 0.1 reshape.89
  11.6 0.7 compare_select_fusion.1
  12.4 0.2 reshape.90
  12.6 1.0 fusion.4
  13.6 0.9 fusion.6
  14.5 19.1 %all_gather.12 = bf16[256,1024]{1,0:T(8,128)(2,1)S(1)} all-gather(bf16[32,1024]{1,0:T(8,128)(2,1)S(1)} %fusion.6), channel_id=1, replica_groups=mesh['ep'=4,'tp'=8] {'tp'}, dimensions={0}, use_global_device_ids=true | all-gather | bytes 589824 | tf_op jit(solution)/shard_map/all_gather | solution.py:40
  33.6 0.5 broadcast_in_dim.7
  34.2 0.4 reshape.111
  34.6 3.2 %scatter_custom_fusion = bf16[1024,1024]{1,0:T(8,128)(2,1)S(1)} fusion(s32[512]{0:T(512)S(1)} %bitcast.42, bf16[512,1024]{1,0:T(8,128)(2,1)S(1)} %reshape.111, bf16[]{:T(256)} %constant.11.clone.1), kind=kCustom, calls=%fused_computation.5 | custom fusion | bytes 2097154 | tf_op jit(solution)/shard_map/scatter | solution.py:17
  37.9 9.8 %all_to_all.28 = bf16[4,32,1024]{2,1,0:T(8,128)(2,1)S(1)} all-to-all(bf16[4,32,1024]{2,1,0:T(8,128)(2,1)S(1)} %bitcast.38), channel_id=1, replica_groups=mesh['ep'=4,'tp'=8] {'ep'}, dimensions={0} | all-to-all | bytes 524288 | tf_op jit(solution)/shard_map/all_to_all | solution.py:45
  47.7 1.7 %fusion.16 = f32[2,64,256]{2,1,0:T(8,128)S(1)} fusion(bf16[2,64,1024]{2,1,0:T(8,128)(2,1)S(1)} %bitcast.36, bf16[2,1024,256]{1,2,0:T(8,128)(2,1)} %all-gather.4.cloned.1.call-done), kind=kOutput, calls=%fused_computation.33 | convolution fusion | flops 67108864 | bytes 1441792 | tf_op jit(solution)/shard_map/erd,edh->erh/dot_general | solution.py:53
  49.4 10.8 %all-gather.6.cloned.1.call-done = bf16[2,1024,256]{1,2,0:T(8,128)(2,1)} async-done(((bf16[2,1024,32]{1,2,0:T(8,128)(2,1)}), bf16[2,1024,256]{1,2,0:T(8,128)(2,1)}) %all-gather.6.cloned.1.call-update) | async-done | bytes 1048592 | tf_op jit(solution)/shard_map/all_gather | solution.py:50
  60.2 23.5 %all-gather.8.cloned.1.call-done = bf16[2,256,1024]{2,1,0:T(8,128)(2,1)} async-done(((bf16[2,32,1024]{2,1,0:T(8,128)(2,1)}), bf16[2,256,1024]{2,1,0:T(8,128)(2,1)}) %all-gather.8.cloned.1.call-update) | async-done | bytes 1048592 | tf_op jit(solution)/shard_map/all_gather | solution.py:51
  83.7 2.2 %convolution_convert_fusion = bf16[2,64,1024]{2,1,0:T(8,128)(2,1)S(1)} fusion(bf16[2,256,1024]{2,1,0:T(8,128)(2,1)} %all-gather.8.cloned.1.call-done, bf16[2,64,1024]{2,1,0:T(8,128)(2,1)S(1)} %bitcast.37, bf16[2,1024,256]{1,2,0:T(8,128)(2,1)} %all-gather.6.cloned.1.call-done, f32[2,64,256]{2,1,0:T(8,128)S(1)} %fusion.16), kind=kOutput, calls=%fused_computation.2 | convolution fusion | flops 134545408 | bytes 2752512 | tf_op jit(solution)/shard_map/erh,ehd->erd/dot_general | solution.py:56
  85.9 1.4 %copy.39 = bf16[2,4,16,1024]{2,1,0,3:T(4,128)(2,1)S(1)} copy(bf16[2,4,16,1024]{3,2,1,0:T(8,128)(2,1)S(1)} %bitcast.40) | data formatting | bytes 524288 | tf_op jit(solution)/shard_map/reshape | solution.py:59
  87.3 2.2 %reshape.121 = bf16[8,2,8192]{2,1,0:T(2,128)(2,1)S(1)} reshape(bf16[1024,2,4,16]{3,2,1,0:T(4,128)(2,1)S(1)} %bitcast.32) | data formatting | bytes 524288
  89.5 12.9 %all_to_all.29 = bf16[8,2,8192]{2,1,0:T(2,128)(2,1)S(1)} all-to-all(bf16[8,2,8192]{2,1,0:T(2,128)(2,1)S(1)} %reshape.121), channel_id=1, replica_groups=mesh['ep'=4,'tp'=8] {'tp'}, dimensions={0} | all-to-all | bytes 524288 | tf_op jit(solution)/shard_map/all_to_all | solution.py:60
  102.3 1.4 %reshape.122 = bf16[1024,2,4,16]{3,2,1,0:T(4,128)(2,1)S(1)} reshape(bf16[8,2,8192]{2,1,0:T(2,128)(2,1)S(1)} %all_to_all.29) | data formatting | bytes 524288
  103.8 2.6 %copy.46 = bf16[2,4,16,8,128]{4,2,3,0,1:T(8,128)(2,1)} copy(bf16[2,4,16,8,128]{2,1,0,4,3:T(4,128)(2,1)S(1)} %bitcast.33) | data formatting | bytes 524288 | tf_op jit(solution)/shard_map/transpose | solution.py:61
  106.4 3.6 %all-to-all-start.2 = ((bf16[4,256,128]{2,1,0:T(8,128)(2,1)}), bf16[4,256,128]{2,1,0:T(8,128)(2,1)S(1)}, u32[]{:S(2)}, u32[]{:S(2)}) async-start(bf16[4,256,128]{2,1,0:T(8,128)(2,1)} %bitcast.15), calls=%async_computation.2 | async-start | bytes 524288 | tf_op jit(solution)/shard_map/all_to_all | solution.py:62
  110.1 0.1 reshape.101
  110.4 4.9 %all-to-all-done.2 = bf16[4,256,128]{2,1,0:T(8,128)(2,1)S(1)} async-done(((bf16[4,256,128]{2,1,0:T(8,128)(2,1)}), bf16[4,256,128]{2,1,0:T(8,128)(2,1)S(1)}, u32[]{:S(2)}, u32[]{:S(2)}) %all-to-all-start.2) | async-done | bytes 262176 | tf_op jit(solution)/shard_map/all_to_all | solution.py:62
  115.3 1.3 %gather_fusion = bf16[512,128]{1,0:T(8,128)(2,1)S(1)} fusion(bf16[1024,128]{1,0:T(8,128)(2,1)S(1)} %bitcast.34, s32[1024]{0:T(1024)S(1)} %pad_clamp_fusion), kind=kCustom, calls=%fused_computation | custom fusion | bytes 264192 | tf_op jit(solution)/shard_map/gather | solution.py:65
  116.7 1.1 fusion.3
  (19 shorter events, 0.8 us)
Async XLA Ops:
  6.5 41.2 %all-gather.4.cloned.1.call-start = ((), (), s32[]{:S(2)}) async-start(), calls=%async_computation.3 | async-start | bytes 1179648 | tf_op jit(solution)/shard_map/all_gather | solution.py:49
  7.3 52.9 %all-gather.6.cloned.1.call-start = ((), (), s32[]{:S(2)}) async-start(), calls=%async_computation.4 | async-start | bytes 1179648 | tf_op jit(solution)/shard_map/all_gather | solution.py:50
  8.0 75.7 %all-gather.8.cloned.1.call-start = ((), (), s32[]{:S(2)}) async-start(), calls=%async_computation.5 | async-start | bytes 1179648 | tf_op jit(solution)/shard_map/all_gather | solution.py:51
  103.8 6.5 %copy-start = (f32[256,2]{0,1:T(2,128)S(1)}, f32[256,2]{0,1:T(2,128)}, u32[]{:S(2)}) copy-start(f32[256,2]{0,1:T(2,128)} %param.10) | copy-start | bytes 6148
  106.4 9.0 %all-to-all-start.2 = ((bf16[4,256,128]{2,1,0:T(8,128)(2,1)}), bf16[4,256,128]{2,1,0:T(8,128)(2,1)S(1)}, u32[]{:S(2)}, u32[]{:S(2)}) async-start(bf16[4,256,128]{2,1,0:T(8,128)(2,1)} %bitcast.15), calls=%async_computation.2 | async-start | bytes 524288 | tf_op jit(solution)/shard_map/all_to_all | solution.py:62
Sparse Core Ops, SparseCore 0:
  8.9 27.6 all-gather.3
  38.3 21.8 all-gather.5
  61.8 21.8 all-gather.7
where the time goes:
time: 125 us; the launch traced here: 124 us
  blocking collectives  41.8 us (33%)
  waiting for transfers between devices  41.3 us (33%)
  local copies, waits for them, and re-layouts  15.3 us (12%)
  between operations  13.3 us (11%)
  other arithmetic  4.95 us (4%)
  matrix products  3.9 us (3%)
  starting transfers between devices  3.66 us (3%)
    all_gather x1, waiting for transfers between devices, body(): lax.all_gather(w_down, 'tp', axis=1, tiled=True)  23.5 us
    all_gather x1, blocking collectives, body(): group = lax.all_gather(normed, 'tp', axis=0, tiled=True)  19.1 us
    all_to_all x1, blocking collectives, body(): lax.all_to_all(produced, 'tp', split_axis=3, concat_axis=2, tiled=True)  12.9 us
    all_gather x1, waiting for transfers between devices, body(): lax.all_gather(w_up, 'tp', axis=2, tiled=True)  10.8 us
    all_to_all x1, blocking collectives, body(): landed = lax.all_to_all(mine, 'ep', split_axis=0, concat_axis=0, tiled=True)  9.78 us
    all_to_all x1, waiting for transfers between devices, body(): lax.all_to_all(leaving, 'ep', split_axis=0, concat_axis=0, tiled=True)  4.92 us
    unnamed x6, local copies, waits for them, and re-layouts  4.55 us
    all_to_all x1, starting transfers between devices, body(): lax.all_to_all(leaving, 'ep', split_axis=0, concat_axis=0, tiled=True)  3.58 us
  transfers between devices with their start and end apart: 4, of which 3 were waited for; matrix products, arithmetic and copies ran while one was open for 10% of the time, Pallas kernels for 0%

commit v1 on v0

--- a/solution.py
+++ b/solution.py
@@ -2,6 +2,7 @@
 import jax.numpy as jnp
 from jax import lax
 from jax.sharding import PartitionSpec as P
+from jax.lax import all_to_all, axis_size
 
 epsilon = 1e-06
 
@@ -57,7 +58,13 @@
         "erh,ehd->erd", hidden, full_down, preferred_element_type=jnp.float32
     ).astype(jnp.bfloat16)
     produced = produced.reshape(local_experts, ep_size, slice_len, model_width)
-    blocks = lax.all_to_all(produced, "tp", split_axis=3, concat_axis=2, tiled=True)
+    field_out = all_to_all(
+        jnp.stack(jnp.split(produced, axis_size("tp"), 3)),
+        concat_axis=0,
+        axis_name="tp",
+        split_axis=0,
+    )
+    blocks = jnp.concatenate(field_out, 2)
     leaving = blocks.transpose(1, 0, 2, 3).reshape(ep_size, local_experts * capacity, columns)
     returned = lax.all_to_all(leaving, "ep", split_axis=0, concat_axis=0, tiled=True).reshape(
         experts * capacity, columns

time: 125 us -> 118 us (0.944)
  local copies, waits for them, and re-layouts: 15.3 us -> 8.68 us
    unnamed x6 -> x11, local copies, waits for them, and re-layouts: 4.55 us -> 1.07 us
    transpose x1, local copies, waits for them, and re-layouts: 2.57 us -> 0.71 us  [body(): blocks.transpose(1, 0, 2, 3)]
    reshape x1 -> x0, local copies, waits for them, and re-layouts: 1.36 us -> none  [body(): produced = produced.reshape(local_experts, ep_size, slice_len, model_width)]
where the time goes in v1:
time: 118 us
  blocking collectives  41.8 us (35%)
  waiting for transfers between devices  41.3 us (35%)
  between operations  13.3 us (11%)
  local copies, waits for them, and re-layouts  8.68 us (7%)
  other arithmetic  4.95 us (4%)
  matrix products  3.9 us (3%)
  starting transfers between devices  3.66 us (3%)
    all_gather x1, waiting for transfers between devices, body(): lax.all_gather(w_down, 'tp', axis=1, tiled=True)  23.5 us
    all_gather x1, blocking collectives, body(): group = lax.all_gather(normed, 'tp', axis=0, tiled=True)  19.1 us
    all_to_all x1, blocking collectives, body(): all_to_all(jnp.stack(jnp.split(produced, axis_size('tp'), 3)), concat_axi...  12.9 us
    all_gather x1, waiting for transfers between devices, body(): lax.all_gather(w_up, 'tp', axis=2, tiled=True)  10.8 us
    all_to_all x1, blocking collectives, body(): landed = lax.all_to_all(mine, 'ep', split_axis=0, concat_axis=0, tiled=True)  9.78 us
    all_to_all x1, waiting for transfers between devices, body(): lax.all_to_all(leaving, 'ep', split_axis=0, concat_axis=0, tiled=True)  4.92 us
    all_to_all x1, starting transfers between devices, body(): lax.all_to_all(leaving, 'ep', split_axis=0, concat_axis=0, tiled=True)  3.58 us
    scatter x1, local copies, waits for them, and re-layouts, fill_buffer(): return buffer.at[flat_target].set(jnp.repeat(group, 2, axis=0))  3.23 us
  transfers between devices with their start and end apart: 4, of which 3 were waited for; matrix products, arithmetic and copies ran while one was open for 10% of the time, Pallas kernels for 0%

profile of v1, /device:TPU:0, one launch (start us, length us, event | category | flops | bytes accessed | tf_op | source)
XLA Modules:
  0.0 117.6 jit_solution(18286929020865902042)
XLA Ops:
  6.5 0.7 all-gather.4.cloned.1.call-update
  7.3 0.7 all-gather.6.cloned.1.call-update
  8.1 0.7 all-gather.8.cloned.1.call-update
  8.7 0.8 copy.45
  9.6 0.1 eq.30
  9.7 0.1 eq.26
  9.9 1.1 reduce-window.6
  11.0 0.2 slice_reduce_fusion
  11.4 0.1 reshape.95
  11.6 0.7 compare_select_fusion.1
  12.3 0.1 copy.48
  12.4 0.2 reshape.96
  12.6 1.0 fusion.4
  13.6 0.9 fusion.6
  14.5 19.1 %all_gather.12 = bf16[256,1024]{1,0:T(8,128)(2,1)S(1)} all-gather(bf16[32,1024]{1,0:T(8,128)(2,1)S(1)} %fusion.6), channel_id=1, replica_groups=mesh['ep'=4,'tp'=8] {'tp'}, dimensions={0}, use_global_device_ids=true | all-gather | bytes 589824 | tf_op jit(solution)/shard_map/all_gather | solution.py:41
  33.6 0.5 broadcast_in_dim.7
  34.2 0.4 reshape.119
  34.6 3.2 %scatter_custom_fusion = bf16[1024,1024]{1,0:T(8,128)(2,1)S(1)} fusion(s32[512]{0:T(512)S(1)} %bitcast.76, bf16[512,1024]{1,0:T(8,128)(2,1)S(1)} %reshape.119, bf16[]{:T(256)} %constant.11.clone.1), kind=kCustom, calls=%fused_computation.5 | custom fusion | bytes 2097154 | tf_op jit(solution)/shard_map/scatter | solution.py:18
  37.9 9.8 %all_to_all.15 = bf16[4,32,1024]{2,1,0:T(8,128)(2,1)S(1)} all-to-all(bf16[4,32,1024]{2,1,0:T(8,128)(2,1)S(1)} %bitcast.64), channel_id=1, replica_groups=mesh['ep'=4,'tp'=8] {'ep'}, dimensions={0} | all-to-all | bytes 524288 | tf_op jit(solution)/shard_map/all_to_all | solution.py:46
  47.7 1.7 %fusion.24 = f32[2,64,256]{2,1,0:T(8,128)S(1)} fusion(bf16[2,64,1024]{2,1,0:T(8,128)(2,1)S(1)} %bitcast.62, bf16[2,1024,256]{1,2,0:T(8,128)(2,1)} %all-gather.4.cloned.1.call-done), kind=kOutput, calls=%fused_computation.49 | convolution fusion | flops 67108864 | bytes 1441792 | tf_op jit(solution)/shard_map/erd,edh->erh/dot_general | solution.py:54
  49.4 10.8 %all-gather.6.cloned.1.call-done = bf16[2,1024,256]{1,2,0:T(8,128)(2,1)} async-done(((bf16[2,1024,32]{1,2,0:T(8,128)(2,1)}), bf16[2,1024,256]{1,2,0:T(8,128)(2,1)}) %all-gather.6.cloned.1.call-update) | async-done | bytes 1048592 | tf_op jit(solution)/shard_map/all_gather | solution.py:51
  60.2 23.5 %all-gather.8.cloned.1.call-done = bf16[2,256,1024]{2,1,0:T(8,128)(2,1)} async-done(((bf16[2,32,1024]{2,1,0:T(8,128)(2,1)}), bf16[2,256,1024]{2,1,0:T(8,128)(2,1)}) %all-gather.8.cloned.1.call-update) | async-done | bytes 1048592 | tf_op jit(solution)/shard_map/all_gather | solution.py:52
  83.7 2.2 %convolution_convert_fusion = bf16[2,64,1024]{2,1,0:T(8,128)(2,1)S(1)} fusion(bf16[2,256,1024]{2,1,0:T(8,128)(2,1)} %all-gather.8.cloned.1.call-done, bf16[2,64,1024]{2,1,0:T(8,128)(2,1)S(1)} %bitcast.63, bf16[2,1024,256]{1,2,0:T(8,128)(2,1)} %all-gather.6.cloned.1.call-done, f32[2,64,256]{2,1,0:T(8,128)S(1)} %fusion.24), kind=kOutput, calls=%fused_computation.2 | convolution fusion | flops 134545408 | bytes 2752512 | tf_op jit(solution)/shard_map/erh,ehd->erd/dot_general | solution.py:57
  86.1 12.9 %all_to_all.16 = bf16[8,2,4,16,128]{4,3,2,1,0:T(8,128)(2,1)S(1)} all-to-all(bf16[8,2,4,16,128]{4,3,2,1,0:T(8,128)(2,1)S(1)} %fusion.13), channel_id=1, replica_groups=mesh['ep'=4,'tp'=8] {'tp'}, dimensions={0} | all-to-all | bytes 524288 | tf_op jit(solution)/shard_map/all_to_all | solution.py:61
  99.0 0.7 copy.51
  99.7 3.6 %all-to-all-start.2 = ((bf16[4,256,128]{2,1,0:T(8,128)(2,1)}), bf16[4,256,128]{2,1,0:T(8,128)(2,1)S(1)}, u32[]{:S(2)}, u32[]{:S(2)}) async-start(bf16[4,256,128]{2,1,0:T(8,128)(2,1)} %bitcast.20), calls=%async_computation.2 | async-start | bytes 524288 | tf_op jit(solution)/shard_map/all_to_all | solution.py:69
  103.3 0.1 copy.52
  103.4 0.1 reshape.109
  103.6 0.1 copy.44
  103.8 4.9 %all-to-all-done.2 = bf16[4,256,128]{2,1,0:T(8,128)(2,1)S(1)} async-done(((bf16[4,256,128]{2,1,0:T(8,128)(2,1)}), bf16[4,256,128]{2,1,0:T(8,128)(2,1)S(1)}, u32[]{:S(2)}, u32[]{:S(2)}) %all-to-all-start.2) | async-done | bytes 262176 | tf_op jit(solution)/shard_map/all_to_all | solution.py:69
  108.7 1.3 %gather_fusion = bf16[512,128]{1,0:T(8,128)(2,1)S(1)} fusion(bf16[1024,128]{1,0:T(8,128)(2,1)S(1)} %bitcast.60, s32[1024]{0:T(1024)S(1)} %pad_clamp_fusion), kind=kCustom, calls=%fused_computation | custom fusion | bytes 264192 | tf_op jit(solution)/shard_map/gather | solution.py:72
  110.0 1.1 fusion.3
  (25 shorter events, 0.5 us)
Async XLA Ops:
  6.5 41.2 %all-gather.4.cloned.1.call-start = ((), (), s32[]{:S(2)}) async-start(), calls=%async_computation.3 | async-start | bytes 1179648 | tf_op jit(solution)/shard_map/all_gather | solution.py:50
  7.3 52.9 %all-gather.6.cloned.1.call-start = ((), (), s32[]{:S(2)}) async-start(), calls=%async_computation.4 | async-start | bytes 1179648 | tf_op jit(solution)/shard_map/all_gather | solution.py:51
  8.0 75.7 %all-gather.8.cloned.1.call-start = ((), (), s32[]{:S(2)}) async-start(), calls=%async_computation.5 | async-start | bytes 1179648 | tf_op jit(solution)/shard_map/all_gather | solution.py:52
  85.9 17.7 %copy-start = (f32[256,2]{0,1:T(2,128)S(1)}, f32[256,2]{0,1:T(2,128)}, u32[]{:S(2)}) copy-start(f32[256,2]{0,1:T(2,128)} %param.10) | copy-start | bytes 6148
  99.7 9.0 %all-to-all-start.2 = ((bf16[4,256,128]{2,1,0:T(8,128)(2,1)}), bf16[4,256,128]{2,1,0:T(8,128)(2,1)S(1)}, u32[]{:S(2)}, u32[]{:S(2)}) async-start(bf16[4,256,128]{2,1,0:T(8,128)(2,1)} %bitcast.20), calls=%async_computation.2 | async-start | bytes 524288 | tf_op jit(solution)/shard_map/all_to_all | solution.py:69
Sparse Core Ops, SparseCore 0:
  8.9 27.6 all-gather.3
  38.3 21.8 all-gather.5
  61.8 21.8 all-gather.7
